TPU v7x, 32 devices: a whole 2x2x4 slice. The times are simulated.
32 devices in a mesh: fs: 8 (over z, y), tp: 4 (over x, core).
Axes of the slice: x: 2, y: 2, z: 4, core: 2. Of those that a mesh axis runs over, the one named last changes fastest.
Arguments:
- stream: bfloat16 [4096, 1024], P(('fs', 'tp')), may hold values from -3 to 3
- mixer_out: bfloat16 [4096, 1024], P(('fs', 'tp')), may hold values from -6 to 6
- ffn_gains: float32 [4, 1024], replicated, may hold values from 0.5 to 1.5
- mixer_gain: float32 [1024], replicated, may hold values from 0.25 to 0.6
- gate_first: bfloat16 [1024, 2816], P('fs', 'tp'), may hold values from -0.1875 to 0.1875
- up_first: bfloat16 [1024, 2816], P('fs', 'tp'), may hold values from -0.1875 to 0.1875
- down_first: bfloat16 [2816, 1024], P('tp', 'fs'), may hold values from -0.109375 to 0.109375
- gate_second: bfloat16 [1024, 2816], P('fs', 'tp'), may hold values from -0.1875 to 0.1875
- up_second: bfloat16 [1024, 2816], P('fs', 'tp'), may hold values from -0.1875 to 0.1875
- down_second: bfloat16 [2816, 1024], P('tp', 'fs'), may hold values from -0.109375 to 0.109375
Outputs:
- layer_out: bfloat16 [4096, 1024], P(('fs', 'tp'))
All inputs are finite; a program needn't handle non-finite values.
Results may differ from a plain program's by a relative error of at most 0.02.
Values may be sent and summed in bfloat16 or wider, within the bound.
A program may use at most 64 MiB of HBM per device.

v0:
```python
import jax
import jax.numpy as jnp
from jax import lax
from jax.sharding import PartitionSpec as P

epsilon = 1e-06
half_weight = 0.5


def over_all(section, axis, dim, apply):
    everything = lax.all_gather(section, axis, axis=dim, tiled=True)
    return apply(everything, jnp.int32(0))


def summed_rows(portion, rows, axis):
    count = rows * lax.axis_size(axis)
    sent = portion(jnp.int32(0), count).astype(jnp.bfloat16)
    return lax.psum_scatter(sent, axis, scatter_dimension=0, tiled=True).astype(jnp.float32)


def rms_rows(values, gain_row):
    widened = values.astype(jnp.float32)
    inverse_rms = lax.rsqrt(jnp.mean(widened * widened, axis=-1, keepdims=True) + epsilon)
    return (widened * inverse_rms * gain_row.astype(jnp.float32)).astype(jnp.bfloat16)


def add_branch(rows, normed_branch, factor):
    return (rows.astype(jnp.float32) + factor * normed_branch.astype(jnp.float32)).astype(
        jnp.bfloat16
    )


def collect_weights(gate_local, up_local, down_local):
    gate_full, up_full = (
        lax.all_gather(gate_local, "fs", axis=0, tiled=True),
        lax.all_gather(up_local, "fs", axis=0, tiled=True),
    )
    down_full = lax.all_gather(down_local, "fs", axis=1, tiled=True)
    return (gate_full, up_full, down_full)


def half_step(rows, gain_pre, gain_post, weight_set):
    gate_full, up_full, down_full = weight_set
    normed = rms_rows(rows, gain_pre)

    def activate(tokens_part, first_row):
        gate_sum = jnp.dot(tokens_part, gate_full, preferred_element_type=jnp.float32)
        up_sum = jnp.dot(tokens_part, up_full, preferred_element_type=jnp.float32)
        return (jax.nn.silu(gate_sum) * up_sum).astype(jnp.bfloat16)

    hidden = over_all(normed, "tp", 0, activate)

    def project(first_row, row_count):
        row_block = lax.dynamic_slice_in_dim(hidden, first_row, row_count, 0)
        return jnp.dot(row_block, down_full, preferred_element_type=jnp.float32)

    branch = summed_rows(project, normed.shape[0], "tp").astype(jnp.bfloat16)
    return add_branch(rows, rms_rows(branch, gain_post), half_weight)


def on_device(
    stream,
    mixer_out,
    ffn_gains,
    mixer_gain,
    gate_first,
    up_first,
    down_first,
    gate_second,
    up_second,
    down_second,
):
    first_set = collect_weights(gate_first, up_first, down_first)
    after_first = half_step(stream, ffn_gains[0], ffn_gains[1], first_set)
    mixed_in = add_branch(after_first, rms_rows(mixer_out, mixer_gain), 1.0)
    second_set = collect_weights(gate_second, up_second, down_second)
    return half_step(mixed_in, ffn_gains[2], ffn_gains[3], second_set)


def solution(mesh):
    in_specs = (
        P(("fs", "tp"), None),
        P(("fs", "tp"), None),
        P(),
        P(),
        P("fs", "tp"),
        P("fs", "tp"),
        P("tp", "fs"),
        P("fs", "tp"),
        P("fs", "tp"),
        P("tp", "fs"),
    )
    out_specs = P(("fs", "tp"), None)
    return jax.shard_map(
        on_device, mesh=mesh, in_specs=in_specs, out_specs=out_specs, check_vma=False
    )
```

profile of v0, /device:TPU:0, one launch (start us, length us, event | category | flops | bytes accessed | tf_op | source)
XLA Modules:
  0.0 376.5 jit_solution(1594553680892777717)
XLA Ops:
  6.5 0.9 fusion.23
  7.4 1.1 fusion.13
  8.5 1.8 fusion.15
  10.3 0.0 all-gather.11.cloned.1.call-start
  10.4 0.7 all-gather.11.cloned.1.call-update
  11.1 0.7 all-gather.13.cloned.1.call-update
  11.9 0.5 all-gather.15.cloned.1.call-update
  12.4 17.5 %all-gather.9.cloned.1.call-done = bf16[512,1024]{1,0:T(8,128)(2,1)} async-done(((bf16[128,1024]{1,0:T(8,128)(2,1)}), bf16[512,1024]{1,0:T(8,128)(2,1)}) %all-gather.9.cloned.1.call-update) | async-done | bytes 1048592 | tf_op jit(solution)/shard_map/all_gather | solution.py:11
  29.9 45.1 %all-gather.11.cloned.1.call-done = bf16[1024,704]{0,1:T(8,128)(2,1)} async-done(((bf16[128,704]{0,1:T(8,128)(2,1)}), bf16[1024,704]{0,1:T(8,128)(2,1)}) %all-gather.11.cloned.1.call-update) | async-done | bytes 1441808 | tf_op jit(solution)/shard_map/all_gather | solution.py:35
  75.0 2.6 fusion.24
  77.6 40.6 %all-gather.13.cloned.1.call-done = bf16[1024,704]{0,1:T(8,128)(2,1)} async-done(((bf16[128,704]{0,1:T(8,128)(2,1)}), bf16[1024,704]{0,1:T(8,128)(2,1)}) %all-gather.13.cloned.1.call-update) | async-done | bytes 1441808 | tf_op jit(solution)/shard_map/all_gather | solution.py:36
  118.2 43.1 %all-gather.15.cloned.1.call-done = bf16[704,1024]{1,0:T(8,128)(2,1)} async-done(((bf16[704,128]{1,0:T(8,128)(2,1)}), bf16[704,1024]{1,0:T(8,128)(2,1)}) %all-gather.15.cloned.1.call-update) | async-done | bytes 1441808 | tf_op jit(solution)/shard_map/all_gather | solution.py:38
  161.3 4.7 %convolution_convert_fusion.1 = bf16[512,1024]{1,0:T(8,128)(2,1)} fusion(bf16[704,1024]{1,0:T(8,128)(2,1)} %all-gather.15.cloned.1.call-done, bf16[512,1024]{1,0:T(8,128)(2,1)S(1)} %copy-done.3, bf16[1024,704]{0,1:T(8,128)(2,1)} %all-gather.13.cloned.1.call-done, f32[512,704]{0,1:T(8,128)S(1)} %fusion.24), kind=kOutput, calls=%fused_computation.1 | convolution fusion | flops 1479081984 | bytes 6422528 | tf_op jit(solution)/shard_map/dot_general | solution.py:55
  166.0 0.0 all-gather.19.cloned.1.call-start
  166.1 0.5 all-gather.19.cloned.1.call-update
  166.7 0.1 fusion.7
  166.8 22.3 %reduce-scatter.3.cloned.1.call-done = bf16[128,1024]{1,0:T(8,128)(2,1)} async-done(((bf16[512,1024]{1,0:T(8,128)(2,1)}), bf16[128,1024]{1,0:T(8,128)(2,1)}) %reduce-scatter.3.cloned.1.call-update) | async-done | bytes 262160 | tf_op jit(solution)/shard_map/reduce_scatter | solution.py:18
  189.2 1.1 fusion.4
  190.3 1.3 fusion.17
  191.6 0.8 fusion.19
  192.5 0.0 all-gather.21.cloned.1.call-start
  192.5 0.7 all-gather.21.cloned.1.call-update
  193.3 0.7 all-gather.23.cloned.1.call-update
  194.0 40.0 %all-gather.19.cloned.1.call-done = bf16[1024,704]{0,1:T(8,128)(2,1)} async-done(((bf16[128,704]{0,1:T(8,128)(2,1)}), bf16[1024,704]{0,1:T(8,128)(2,1)}) %all-gather.19.cloned.1.call-update) | async-done | bytes 1441808 | tf_op jit(solution)/shard_map/all_gather | solution.py:35
  234.1 16.5 %all-gather.17.cloned.1.call-done = bf16[512,1024]{1,0:T(8,128)(2,1)} async-done(((bf16[128,1024]{1,0:T(8,128)(2,1)}), bf16[512,1024]{1,0:T(8,128)(2,1)}) %all-gather.17.cloned.1.call-update) | async-done | bytes 1048592 | tf_op jit(solution)/shard_map/all_gather | solution.py:11
  250.5 2.7 fusion.25
  253.2 42.3 %all-gather.21.cloned.1.call-done = bf16[1024,704]{0,1:T(8,128)(2,1)} async-done(((bf16[128,704]{0,1:T(8,128)(2,1)}), bf16[1024,704]{0,1:T(8,128)(2,1)}) %all-gather.21.cloned.1.call-update) | async-done | bytes 1441808 | tf_op jit(solution)/shard_map/all_gather | solution.py:36
  295.6 43.2 %all-gather.23.cloned.1.call-done = bf16[704,1024]{1,0:T(8,128)(2,1)} async-done(((bf16[704,128]{1,0:T(8,128)(2,1)}), bf16[704,1024]{1,0:T(8,128)(2,1)}) %all-gather.23.cloned.1.call-update) | async-done | bytes 1441808 | tf_op jit(solution)/shard_map/all_gather | solution.py:38
  338.8 4.7 %convolution_convert_fusion = bf16[512,1024]{1,0:T(8,128)(2,1)} fusion(bf16[704,1024]{1,0:T(8,128)(2,1)} %all-gather.23.cloned.1.call-done, bf16[512,1024]{1,0:T(8,128)(2,1)S(1)} %copy-done.4, bf16[1024,704]{0,1:T(8,128)(2,1)} %all-gather.21.cloned.1.call-done, f32[512,704]{0,1:T(8,128)S(1)} %fusion.25), kind=kOutput, calls=%fused_computation | convolution fusion | flops 1479081984 | bytes 6422528 | tf_op jit(solution)/shard_map/dot_general | solution.py:55
  343.6 23.1 %reduce-scatter.5.cloned.1.call-done = bf16[128,1024]{1,0:T(8,128)(2,1)} async-done(((bf16[512,1024]{1,0:T(8,128)(2,1)}), bf16[128,1024]{1,0:T(8,128)(2,1)}) %reduce-scatter.5.cloned.1.call-update) | async-done | bytes 262160 | tf_op jit(solution)/shard_map/reduce_scatter | solution.py:18
  366.7 1.1 fusion.10
  367.8 1.8 fusion.20
  (26 shorter events, 0.4 us)
Async XLA Ops:
  6.5 23.4 %all-gather.9.cloned.1.call-start = ((), (), s32[]{:S(2)}) async-start(), calls=%async_computation.2 | async-start | bytes 1310720 | tf_op jit(solution)/shard_map/all_gather | solution.py:11
  10.3 64.6 %all-gather.11.cloned.1.call-start = ((), (), s32[]{:S(2)}) async-start(), calls=%async_computation.3 | async-start | bytes 1622016 | tf_op jit(solution)/shard_map/all_gather | solution.py:35
  11.1 107.1 %all-gather.13.cloned.1.call-start = ((), (), s32[]{:S(2)}) async-start(), calls=%async_computation.4 | async-start | bytes 1622016 | tf_op jit(solution)/shard_map/all_gather | solution.py:36
  11.8 149.5 %all-gather.15.cloned.1.call-start = ((), (), s32[]{:S(2)}) async-start(), calls=%async_computation.5 | async-start | bytes 1622016 | tf_op jit(solution)/shard_map/all_gather | solution.py:38
  12.4 176.8 %reduce-scatter.3.cloned.1.call-start = ((), (), s32[]{:S(2)}) async-start(), calls=%async_computation.6 | async-start | bytes 1310720 | tf_op jit(solution)/shard_map/reduce_scatter | solution.py:18
  29.9 131.4 %copy-start.3 = (bf16[512,1024]{1,0:T(8,128)(2,1)S(1)}, bf16[512,1024]{1,0:T(8,128)(2,1)}, u32[]{:S(2)}) copy-start(bf16[512,1024]{1,0:T(8,128)(2,1)} %all-gather.9.cloned.1.call-done) | copy-start | bytes 3145732
  77.6 89.1 %copy-start.1 = (bf16[128,1024]{1,0:T(8,128)(2,1)S(1)}, bf16[128,1024]{1,0:T(8,128)(2,1)}, u32[]{:S(2)}) copy-start(bf16[128,1024]{1,0:T(8,128)(2,1)} %param.11) | copy-start | bytes 786436
  166.0 24.2 %copy-start = (bf16[128,1024]{1,0:T(8,128)(2,1)S(1)}, bf16[128,1024]{1,0:T(8,128)(2,1)}, u32[]{:S(2)}) copy-start(bf16[128,1024]{1,0:T(8,128)(2,1)} %param.10) | copy-start | bytes 786436
  166.0 24.3 %copy-start.2 = (f32[1024]{0:T(1024)S(1)}, f32[1024]{0:T(1024)}, u32[]{:S(2)}) copy-start(f32[1024]{0:T(1024)} %param.13) | copy-start | bytes 12292
  166.0 68.0 %all-gather.19.cloned.1.call-start = ((), (), s32[]{:S(2)}) async-start(), calls=%async_computation.8 | async-start | bytes 1622016 | tf_op jit(solution)/shard_map/all_gather | solution.py:35
  166.6 83.9 %all-gather.17.cloned.1.call-start = ((), (), s32[]{:S(2)}) async-start(), calls=%async_computation.7 | async-start | bytes 1310720 | tf_op jit(solution)/shard_map/all_gather | solution.py:11
  192.5 103.1 %all-gather.21.cloned.1.call-start = ((), (), s32[]{:S(2)}) async-start(), calls=%async_computation.9 | async-start | bytes 1622016 | tf_op jit(solution)/shard_map/all_gather | solution.py:36
  193.2 145.6 %all-gather.23.cloned.1.call-start = ((), (), s32[]{:S(2)}) async-start(), calls=%async_computation.10 | async-start | bytes 1622016 | tf_op jit(solution)/shard_map/all_gather | solution.py:38
  194.0 172.7 %reduce-scatter.5.cloned.1.call-start = ((), (), s32[]{:S(2)}) async-start(), calls=%async_computation.11 | async-start | bytes 1310720 | tf_op jit(solution)/shard_map/reduce_scatter | solution.py:18
  250.5 88.3 %copy-start.4 = (bf16[512,1024]{1,0:T(8,128)(2,1)S(1)}, bf16[512,1024]{1,0:T(8,128)(2,1)}, u32[]{:S(2)}) copy-start(bf16[512,1024]{1,0:T(8,128)(2,1)} %all-gather.17.cloned.1.call-done) | copy-start | bytes 3145732
Sparse Core Ops, SparseCore 0:
  10.4 19.4 all-gather.8
  31.9 42.9 all-gather.10
  77.0 41.1 all-gather.12
  120.1 41.1 all-gather.14
  166.2 22.9 reduce-scatter.2
  191.1 42.9 all-gather.18
  235.6 14.8 all-gather.16
  252.6 42.9 all-gather.20
  297.6 41.1 all-gather.22
  343.7 22.9 reduce-scatter.4
where the time goes:
time: 377 us; the launch traced here: 376 us
  waiting for transfers between devices  338 us (90%)
  matrix products  14.8 us (4%)
  between operations  13.6 us (4%)
  other arithmetic  9.24 us (2%)
    all_gather x2, waiting for transfers between devices, collect_weights(): down_full = lax.all_gather(down_local, 'fs', axis=1, tiled=True)  86.3 us
    all_gather x2, waiting for transfers between devices, collect_weights(): lax.all_gather(gate_local, 'fs', axis=0, tiled=True)  85.1 us
    all_gather x2, waiting for transfers between devices, collect_weights(): lax.all_gather(up_local, 'fs', axis=0, tiled=True)  82.9 us
    reduce_scatter x2, waiting for transfers between devices, summed_rows(): lax.psum_scatter(sent, axis, scatter_dimension=0, tiled=True)  45.5 us
    all_gather x2, waiting for transfers between devices, over_all(): everything = lax.all_gather(section, axis, axis=dim, tiled=True)  33.9 us
    dot_general x2, matrix products, project(): return jnp.dot(row_block, down_full, preferred_element_type=jnp.float32)  9.42 us
  transfers between devices with their start and end apart: 10, of which 10 were waited for; matrix products, arithmetic and copies ran while one was open for 2% of the time, Pallas kernels for 0%

commit v1 on v0

--- a/solution.py
+++ b/solution.py
@@ -35,7 +35,13 @@
         lax.all_gather(gate_local, "fs", axis=0, tiled=True),
         lax.all_gather(up_local, "fs", axis=0, tiled=True),
     )
-    down_full = lax.all_gather(down_local, "fs", axis=1, tiled=True)
+    size = lax.axis_size("fs")
+    current, blocks = (down_local, [down_local])
+    for _ in range(size - 1):
+        current = lax.ppermute(current, "fs", [(i, (i + 1) % size) for i in range(size)])
+        blocks.insert(0, current)
+    row_of_blocks = jnp.concatenate(blocks, axis=1)
+    down_full = jnp.roll(row_of_blocks, (lax.axis_index("fs") + 1) * down_local.shape[1], axis=1)
     return (gate_full, up_full, down_full)
 
 

time: 377 us -> 309 us (0.82)
  waiting for transfers between devices: 338 us -> 261 us
  starting transfers between devices: 0.35 us -> 4.88 us
    ppermute x0 -> x14, waiting for transfers between devices: none -> 134 us  [collect_weights(): lax.ppermute(current, 'fs', [(i, (i + 1) % size) for i in range(size)])]
    all_gather x2 -> x0, waiting for transfers between devices: 86.3 us -> none  [collect_weights(): down_full = lax.all_gather(down_local, 'fs', axis=1, tiled=True)]
    all_gather x2, waiting for transfers between devices: 85.1 us -> 0.04 us  [collect_weights(): lax.all_gather(gate_local, 'fs', axis=0, tiled=True)]
    all_gather x2, waiting for transfers between devices: 33.9 us -> 0.04 us  [over_all(): everything = lax.all_gather(section, axis, axis=dim, tiled=True)]
    ppermute x0 -> x14, starting transfers between devices: none -> 4.6 us  [collect_weights(): lax.ppermute(current, 'fs', [(i, (i + 1) % size) for i in range(size)])]
    all_gather x2, waiting for transfers between devices: 82.9 us -> 79 us  [collect_weights(): lax.all_gather(up_local, 'fs', axis=0, tiled=True)]
  transfers between devices with their start and end apart: 10 -> 22, of which waited for: 10 -> 18; matrix products, arithmetic and copies ran while one was open for 2% -> 4% of each run, Pallas kernels for 0% -> 0%
where the time goes in v1:
time: 309 us
  waiting for transfers between devices  261 us (84%)
  matrix products  17.6 us (6%)
  between operations  13.7 us (4%)
  other arithmetic  9.24 us (3%)
  starting transfers between devices  4.88 us (2%)
    ppermute x14, waiting for transfers between devices, collect_weights(): lax.ppermute(current, 'fs', [(i, (i + 1) % size) for i in range(size)])  134 us
    all_gather x2, waiting for transfers between devices, collect_weights(): lax.all_gather(up_local, 'fs', axis=0, tiled=True)  79 us
    reduce_scatter x2, waiting for transfers between devices, summed_rows(): lax.psum_scatter(sent, axis, scatter_dimension=0, tiled=True)  45.4 us
    dot_general x2, matrix products, project(): return jnp.dot(row_block, down_full, preferred_element_type=jnp.float32)  10 us
    dot_general x2, matrix products, activate(): jnp.dot(tokens_part, gate_full, preferred_element_type=jnp.float32)  7.55 us
  transfers between devices with their start and end apart: 22, of which 18 were waited for; matrix products, arithmetic and copies ran while one was open for 4% of the time, Pallas kernels for 0%

profile of v1, /device:TPU:0, one launch (start us, length us, event | category | flops | bytes accessed | tf_op | source)
XLA Modules:
  0.0 308.5 jit_solution(17904591484580359883)
XLA Ops:
  6.5 0.9 fusion.29
  7.4 1.1 fusion.15
  8.5 1.8 fusion.17
  11.9 3.0 collective-permute-start
  14.9 7.6 %collective-permute-done = bf16[704,128]{1,0:T(8,128)(2,1)S(1)} collective-permute-done((bf16[704,128]{1,0:T(8,128)(2,1)S(1)}, bf16[704,128]{1,0:T(8,128)(2,1)S(1)}, u32[]{:S(2)}, u32[]{:S(2)}) %collective-permute-start) | collective-permute-done | bytes 180256 | tf_op jit(solution)/shard_map/ppermute | solution.py:41
  22.5 8.4 %collective-permute-done.1 = bf16[704,128]{1,0:T(8,128)(2,1)S(1)} collective-permute-done((bf16[704,128]{1,0:T(8,128)(2,1)S(1)}, bf16[704,128]{1,0:T(8,128)(2,1)S(1)}, u32[]{:S(2)}, u32[]{:S(2)}) %collective-permute-start.1) | collective-permute-done | bytes 180256 | tf_op jit(solution)/shard_map/ppermute | solution.py:41
  30.9 8.2 %collective-permute-done.2 = bf16[704,128]{1,0:T(8,128)(2,1)S(1)} collective-permute-done((bf16[704,128]{1,0:T(8,128)(2,1)S(1)}, bf16[704,128]{1,0:T(8,128)(2,1)S(1)}, u32[]{:S(2)}, u32[]{:S(2)}) %collective-permute-start.2) | collective-permute-done | bytes 180256 | tf_op jit(solution)/shard_map/ppermute | solution.py:41
  39.1 10.7 %collective-permute-done.3 = bf16[704,128]{1,0:T(8,128)(2,1)S(1)} collective-permute-done((bf16[704,128]{1,0:T(8,128)(2,1)S(1)}, bf16[704,128]{1,0:T(8,128)(2,1)S(1)}, u32[]{:S(2)}, u32[]{:S(2)}) %collective-permute-start.3) | collective-permute-done | bytes 180256 | tf_op jit(solution)/shard_map/ppermute | solution.py:41
  49.9 8.3 %collective-permute-done.4 = bf16[704,128]{1,0:T(8,128)(2,1)S(1)} collective-permute-done((bf16[704,128]{1,0:T(8,128)(2,1)S(1)}, bf16[704,128]{1,0:T(8,128)(2,1)S(1)}, u32[]{:S(2)}, u32[]{:S(2)}) %collective-permute-start.4) | collective-permute-done | bytes 180256 | tf_op jit(solution)/shard_map/ppermute | solution.py:41
  58.2 11.0 %collective-permute-done.5 = bf16[704,128]{1,0:T(8,128)(2,1)S(1)} collective-permute-done((bf16[704,128]{1,0:T(8,128)(2,1)S(1)}, bf16[704,128]{1,0:T(8,128)(2,1)S(1)}, u32[]{:S(2)}, u32[]{:S(2)}) %collective-permute-start.5) | collective-permute-done | bytes 180256 | tf_op jit(solution)/shard_map/ppermute | solution.py:41
  69.2 12.1 %collective-permute-done.6 = bf16[704,128]{1,0:T(8,128)(2,1)S(1)} collective-permute-done((bf16[704,128]{1,0:T(8,128)(2,1)S(1)}, bf16[704,128]{1,0:T(8,128)(2,1)S(1)}, u32[]{:S(2)}, u32[]{:S(2)}) %collective-permute-start.6) | collective-permute-done | bytes 180256 | tf_op jit(solution)/shard_map/ppermute | solution.py:41
  81.9 3.7 %fusion.30 = f32[512,704]{0,1:T(8,128)} fusion(bf16[512,1024]{1,0:T(8,128)(2,1)} %all-gather.7.cloned.1.call-done, bf16[1024,704]{0,1:T(8,128)(2,1)} %all-gather.9.cloned.1.call-done), kind=kOutput, calls=%fused_computation.70 | convolution fusion | flops 738197504 | bytes 3932160 | tf_op jit(solution)/shard_map/dot_general | solution.py:53
  85.6 40.5 %all-gather.11.cloned.1.call-done = bf16[1024,704]{0,1:T(8,128)(2,1)} async-done(((bf16[128,704]{0,1:T(8,128)(2,1)}), bf16[1024,704]{0,1:T(8,128)(2,1)}) %all-gather.11.cloned.1.call-update) | async-done | bytes 1441808 | tf_op jit(solution)/shard_map/all_gather | solution.py:36
  126.1 5.2 %convolution_convert_fusion.1 = bf16[512,1024]{1,0:T(8,128)(2,1)} fusion(s32[]{:T(128)S(6)} %select_n.13, bf16[704,1024]{1,0:T(8,128)(2,1)S(1)} %constant_dynamic-update-slice_fusion, bf16[512,1024]{1,0:T(8,128)(2,1)} %all-gather.7.cloned.1.call-done, bf16[1024,704]{0,1:T(8,128)(2,1)} %all-gather.11.cloned.1.call-done, f32[512,704]{0,1:T(8,128)} %fusion.30), kind=kOutput, calls=%fused_computation.5 | convolution fusion | flops 1481965568 | bytes 6422532 | tf_op jit(solution)/shard_map/dot_general | solution.py:61
  132.1 22.3 %reduce-scatter.3.cloned.1.call-done = bf16[128,1024]{1,0:T(8,128)(2,1)} async-done(((bf16[512,1024]{1,0:T(8,128)(2,1)}), bf16[128,1024]{1,0:T(8,128)(2,1)}) %reduce-scatter.3.cloned.1.call-update) | async-done | bytes 262160 | tf_op jit(solution)/shard_map/reduce_scatter | solution.py:18
  154.5 1.1 fusion.6
  155.6 1.3 fusion.19
  156.9 0.8 fusion.21
  158.6 1.5 collective-permute-start.7
  160.1 7.4 %collective-permute-done.7 = bf16[704,128]{1,0:T(8,128)(2,1)S(1)} collective-permute-done((bf16[704,128]{1,0:T(8,128)(2,1)S(1)}, bf16[704,128]{1,0:T(8,128)(2,1)S(1)}, u32[]{:S(2)}, u32[]{:S(2)}) %collective-permute-start.7) | collective-permute-done | bytes 180256 | tf_op jit(solution)/shard_map/ppermute | solution.py:41
  167.5 9.9 %collective-permute-done.8 = bf16[704,128]{1,0:T(8,128)(2,1)S(1)} collective-permute-done((bf16[704,128]{1,0:T(8,128)(2,1)S(1)}, bf16[704,128]{1,0:T(8,128)(2,1)S(1)}, u32[]{:S(2)}, u32[]{:S(2)}) %collective-permute-start.8) | collective-permute-done | bytes 180256 | tf_op jit(solution)/shard_map/ppermute | solution.py:41
  177.5 8.2 %collective-permute-done.9 = bf16[704,128]{1,0:T(8,128)(2,1)S(1)} collective-permute-done((bf16[704,128]{1,0:T(8,128)(2,1)S(1)}, bf16[704,128]{1,0:T(8,128)(2,1)S(1)}, u32[]{:S(2)}, u32[]{:S(2)}) %collective-permute-start.9) | collective-permute-done | bytes 180256 | tf_op jit(solution)/shard_map/ppermute | solution.py:41
  185.7 12.5 %collective-permute-done.10 = bf16[704,128]{1,0:T(8,128)(2,1)S(1)} collective-permute-done((bf16[704,128]{1,0:T(8,128)(2,1)S(1)}, bf16[704,128]{1,0:T(8,128)(2,1)S(1)}, u32[]{:S(2)}, u32[]{:S(2)}) %collective-permute-start.10) | collective-permute-done | bytes 180256 | tf_op jit(solution)/shard_map/ppermute | solution.py:41
  198.2 12.3 %collective-permute-done.11 = bf16[704,128]{1,0:T(8,128)(2,1)S(1)} collective-permute-done((bf16[704,128]{1,0:T(8,128)(2,1)S(1)}, bf16[704,128]{1,0:T(8,128)(2,1)S(1)}, u32[]{:S(2)}, u32[]{:S(2)}) %collective-permute-start.11) | collective-permute-done | bytes 180256 | tf_op jit(solution)/shard_map/ppermute | solution.py:41
  210.5 9.3 %collective-permute-done.12 = bf16[704,128]{1,0:T(8,128)(2,1)S(1)} collective-permute-done((bf16[704,128]{1,0:T(8,128)(2,1)S(1)}, bf16[704,128]{1,0:T(8,128)(2,1)S(1)}, u32[]{:S(2)}, u32[]{:S(2)}) %collective-permute-start.12) | collective-permute-done | bytes 180256 | tf_op jit(solution)/shard_map/ppermute | solution.py:41
  219.7 8.2 %collective-permute-done.13 = bf16[704,128]{1,0:T(8,128)(2,1)S(1)} collective-permute-done((bf16[704,128]{1,0:T(8,128)(2,1)S(1)}, bf16[704,128]{1,0:T(8,128)(2,1)S(1)}, u32[]{:S(2)}, u32[]{:S(2)}) %collective-permute-start.13) | collective-permute-done | bytes 180256 | tf_op jit(solution)/shard_map/ppermute | solution.py:41
  228.5 3.8 %fusion.31 = f32[512,704]{0,1:T(8,128)} fusion(bf16[512,1024]{1,0:T(8,128)(2,1)} %all-gather.13.cloned.1.call-done, bf16[1024,704]{0,1:T(8,128)(2,1)} %all-gather.15.cloned.1.call-done), kind=kOutput, calls=%fused_computation.71 | convolution fusion | flops 738197504 | bytes 3932160 | tf_op jit(solution)/shard_map/dot_general | solution.py:53
  232.3 38.5 %all-gather.17.cloned.1.call-done = bf16[1024,704]{0,1:T(8,128)(2,1)} async-done(((bf16[128,704]{0,1:T(8,128)(2,1)}), bf16[1024,704]{0,1:T(8,128)(2,1)}) %all-gather.17.cloned.1.call-update) | async-done | bytes 1441808 | tf_op jit(solution)/shard_map/all_gather | solution.py:36
  270.8 4.9 %convolution_convert_fusion = bf16[512,1024]{1,0:T(8,128)(2,1)} fusion(s32[]{:T(128)S(6)} %select_n.13, bf16[704,1024]{1,0:T(8,128)(2,1)S(1)} %constant_dynamic-update-slice_fusion.8, bf16[512,1024]{1,0:T(8,128)(2,1)S(1)} %copy-done.5, bf16[1024,704]{0,1:T(8,128)(2,1)} %all-gather.17.cloned.1.call-done, f32[512,704]{0,1:T(8,128)} %fusion.31), kind=kOutput, calls=%fused_computation.4 | convolution fusion | flops 1481965568 | bytes 6422532 | tf_op jit(solution)/shard_map/dot_general | solution.py:61
  275.7 23.1 %reduce-scatter.5.cloned.1.call-done = bf16[128,1024]{1,0:T(8,128)(2,1)} async-done(((bf16[512,1024]{1,0:T(8,128)(2,1)}), bf16[128,1024]{1,0:T(8,128)(2,1)}) %reduce-scatter.5.cloned.1.call-update) | async-done | bytes 262160 | tf_op jit(solution)/shard_map/reduce_scatter | solution.py:18
  298.8 1.1 fusion.12
  299.8 1.8 fusion.22
  (66 shorter events, 4.1 us)
Async XLA Ops:
  6.5 5.3 %copy-start.2 = (bf16[704,128]{1,0:T(8,128)(2,1)S(1)}, bf16[704,128]{1,0:T(8,128)(2,1)}, u32[]{:S(2)}) copy-start(bf16[704,128]{1,0:T(8,128)(2,1)} %param.18) | copy-start | bytes 540676
  6.5 75.3 %all-gather.7.cloned.1.call-start = ((), (), s32[]{:S(2)}) async-start(), calls=%async_computation.2 | async-start | bytes 1310720 | tf_op jit(solution)/shard_map/all_gather | solution.py:11
  10.3 71.5 %all-gather.9.cloned.1.call-start = ((), (), s32[]{:S(2)}) async-start(), calls=%async_computation.3 | async-start | bytes 1622016 | tf_op jit(solution)/shard_map/all_gather | solution.py:35
  11.1 115.1 %all-gather.11.cloned.1.call-start = ((), (), s32[]{:S(2)}) async-start(), calls=%async_computation.4 | async-start | bytes 1622016 | tf_op jit(solution)/shard_map/all_gather | solution.py:36
  11.8 142.7 %reduce-scatter.3.cloned.1.call-start = ((), (), s32[]{:S(2)}) async-start(), calls=%async_computation.5 | async-start | bytes 1310720 | tf_op jit(solution)/shard_map/reduce_scatter | solution.py:18
  11.9 10.6 %collective-permute-start = (bf16[704,128]{1,0:T(8,128)(2,1)S(1)}, bf16[704,128]{1,0:T(8,128)(2,1)S(1)}, u32[]{:S(2)}, u32[]{:S(2)}) collective-permute-start(bf16[704,128]{1,0:T(8,128)(2,1)S(1)} %copy-done.2), channel_id=1, source_target_pairs={{0,4},{4,8},{8,12},{12,16},{16,20},{20,24},{24,28},{28,0},{1,5},{5... | collective-permute-start | bytes 540680 | tf_op jit(solution)/shard_map/ppermute | solution.py:41
  22.5 8.4 %collective-permute-start.1 = (bf16[704,128]{1,0:T(8,128)(2,1)S(1)}, bf16[704,128]{1,0:T(8,128)(2,1)S(1)}, u32[]{:S(2)}, u32[]{:S(2)}) collective-permute-start(bf16[704,128]{1,0:T(8,128)(2,1)S(1)} %collective-permute-done), channel_id=1, source_target_pairs={{0,4},{4,8},{8,12},{12,16},{16,20},{20,24},{24,28},{28,0},{1,5},{5... | collective-permute-start | bytes 540680 | tf_op jit(solution)/shard_map/ppermute | solution.py:41
  30.9 8.2 %collective-permute-start.2 = (bf16[704,128]{1,0:T(8,128)(2,1)S(1)}, bf16[704,128]{1,0:T(8,128)(2,1)S(1)}, u32[]{:S(2)}, u32[]{:S(2)}) collective-permute-start(bf16[704,128]{1,0:T(8,128)(2,1)S(1)} %collective-permute-done.1), channel_id=1, source_target_pairs={{0,4},{4,8},{8,12},{12,16},{16,20},{20,24},{24,28},{28,0},{1,5},{5... | collective-permute-start | bytes 540680 | tf_op jit(solution)/shard_map/ppermute | solution.py:41
  39.1 10.8 %collective-permute-start.3 = (bf16[704,128]{1,0:T(8,128)(2,1)S(1)}, bf16[704,128]{1,0:T(8,128)(2,1)S(1)}, u32[]{:S(2)}, u32[]{:S(2)}) collective-permute-start(bf16[704,128]{1,0:T(8,128)(2,1)S(1)} %collective-permute-done.2), channel_id=1, source_target_pairs={{0,4},{4,8},{8,12},{12,16},{16,20},{20,24},{24,28},{28,0},{1,5},{5... | collective-permute-start | bytes 540680 | tf_op jit(solution)/shard_map/ppermute | solution.py:41
  49.9 8.3 %collective-permute-start.4 = (bf16[704,128]{1,0:T(8,128)(2,1)S(1)}, bf16[704,128]{1,0:T(8,128)(2,1)S(1)}, u32[]{:S(2)}, u32[]{:S(2)}) collective-permute-start(bf16[704,128]{1,0:T(8,128)(2,1)S(1)} %collective-permute-done.3), channel_id=1, source_target_pairs={{0,4},{4,8},{8,12},{12,16},{16,20},{20,24},{24,28},{28,0},{1,5},{5... | collective-permute-start | bytes 540680 | tf_op jit(solution)/shard_map/ppermute | solution.py:41
  58.2 11.0 %collective-permute-start.5 = (bf16[704,128]{1,0:T(8,128)(2,1)S(1)}, bf16[704,128]{1,0:T(8,128)(2,1)S(1)}, u32[]{:S(2)}, u32[]{:S(2)}) collective-permute-start(bf16[704,128]{1,0:T(8,128)(2,1)S(1)} %collective-permute-done.4), channel_id=1, source_target_pairs={{0,4},{4,8},{8,12},{12,16},{16,20},{20,24},{24,28},{28,0},{1,5},{5... | collective-permute-start | bytes 540680 | tf_op jit(solution)/shard_map/ppermute | solution.py:41
  69.2 12.1 %collective-permute-start.6 = (bf16[704,128]{1,0:T(8,128)(2,1)S(1)}, bf16[704,128]{1,0:T(8,128)(2,1)S(1)}, u32[]{:S(2)}, u32[]{:S(2)}) collective-permute-start(bf16[704,128]{1,0:T(8,128)(2,1)S(1)} %collective-permute-done.5), channel_id=1, source_target_pairs={{0,4},{4,8},{8,12},{12,16},{16,20},{20,24},{24,28},{28,0},{1,5},{5... | collective-permute-start | bytes 540680 | tf_op jit(solution)/shard_map/ppermute | solution.py:41
  85.6 46.4 %copy-start.1 = (bf16[128,1024]{1,0:T(8,128)(2,1)S(1)}, bf16[128,1024]{1,0:T(8,128)(2,1)}, u32[]{:S(2)}) copy-start(bf16[128,1024]{1,0:T(8,128)(2,1)} %param.13) | copy-start | bytes 786436
  131.3 24.3 %copy-start = (bf16[128,1024]{1,0:T(8,128)(2,1)S(1)}, bf16[128,1024]{1,0:T(8,128)(2,1)}, u32[]{:S(2)}) copy-start(bf16[128,1024]{1,0:T(8,128)(2,1)} %param.12) | copy-start | bytes 786436
  131.3 24.3 %copy-start.4 = (f32[1024]{0:T(1024)S(1)}, f32[1024]{0:T(1024)}, u32[]{:S(2)}) copy-start(f32[1024]{0:T(1024)} %param.15) | copy-start | bytes 12292
  131.3 27.3 %copy-start.3 = (bf16[704,128]{1,0:T(8,128)(2,1)S(1)}, bf16[704,128]{1,0:T(8,128)(2,1)}, u32[]{:S(2)}) copy-start(bf16[704,128]{1,0:T(8,128)(2,1)} %param.21) | copy-start | bytes 540676
  131.3 97.1 %all-gather.15.cloned.1.call-start = ((), (), s32[]{:S(2)}) async-start(), calls=%async_computation.7 | async-start | bytes 1622016 | tf_op jit(solution)/shard_map/all_gather | solution.py:35
  131.9 96.5 %all-gather.13.cloned.1.call-start = ((), (), s32[]{:S(2)}) async-start(), calls=%async_computation.6 | async-start | bytes 1310720 | tf_op jit(solution)/shard_map/all_gather | solution.py:11
  157.8 113.0 %all-gather.17.cloned.1.call-start = ((), (), s32[]{:S(2)}) async-start(), calls=%async_computation.8 | async-start | bytes 1622016 | tf_op jit(solution)/shard_map/all_gather | solution.py:36
  158.6 140.2 %reduce-scatter.5.cloned.1.call-start = ((), (), s32[]{:S(2)}) async-start(), calls=%async_computation.9 | async-start | bytes 1310720 | tf_op jit(solution)/shard_map/reduce_scatter | solution.py:18
  158.6 8.9 %collective-permute-start.7 = (bf16[704,128]{1,0:T(8,128)(2,1)S(1)}, bf16[704,128]{1,0:T(8,128)(2,1)S(1)}, u32[]{:S(2)}, u32[]{:S(2)}) collective-permute-start(bf16[704,128]{1,0:T(8,128)(2,1)S(1)} %copy-done.3), channel_id=1, source_target_pairs={{0,4},{4,8},{8,12},{12,16},{16,20},{20,24},{24,28},{28,0},{1,5},{5... | collective-permute-start | bytes 540680 | tf_op jit(solution)/shard_map/ppermute | solution.py:41
  167.5 9.9 %collective-permute-start.8 = (bf16[704,128]{1,0:T(8,128)(2,1)S(1)}, bf16[704,128]{1,0:T(8,128)(2,1)S(1)}, u32[]{:S(2)}, u32[]{:S(2)}) collective-permute-start(bf16[704,128]{1,0:T(8,128)(2,1)S(1)} %collective-permute-done.7), channel_id=1, source_target_pairs={{0,4},{4,8},{8,12},{12,16},{16,20},{20,24},{24,28},{28,0},{1,5},{5... | collective-permute-start | bytes 540680 | tf_op jit(solution)/shard_map/ppermute | solution.py:41
  177.5 8.2 %collective-permute-start.9 = (bf16[704,128]{1,0:T(8,128)(2,1)S(1)}, bf16[704,128]{1,0:T(8,128)(2,1)S(1)}, u32[]{:S(2)}, u32[]{:S(2)}) collective-permute-start(bf16[704,128]{1,0:T(8,128)(2,1)S(1)} %collective-permute-done.8), channel_id=1, source_target_pairs={{0,4},{4,8},{8,12},{12,16},{16,20},{20,24},{24,28},{28,0},{1,5},{5... | collective-permute-start | bytes 540680 | tf_op jit(solution)/shard_map/ppermute | solution.py:41
  185.7 12.5 %collective-permute-start.10 = (bf16[704,128]{1,0:T(8,128)(2,1)S(1)}, bf16[704,128]{1,0:T(8,128)(2,1)S(1)}, u32[]{:S(2)}, u32[]{:S(2)}) collective-permute-start(bf16[704,128]{1,0:T(8,128)(2,1)S(1)} %collective-permute-done.9), channel_id=1, source_target_pairs={{0,4},{4,8},{8,12},{12,16},{16,20},{20,24},{24,28},{28,0},{1,5},{5... | collective-permute-start | bytes 540680 | tf_op jit(solution)/shard_map/ppermute | solution.py:41
  198.2 12.3 %collective-permute-start.11 = (bf16[704,128]{1,0:T(8,128)(2,1)S(1)}, bf16[704,128]{1,0:T(8,128)(2,1)S(1)}, u32[]{:S(2)}, u32[]{:S(2)}) collective-permute-start(bf16[704,128]{1,0:T(8,128)(2,1)S(1)} %collective-permute-done.10), channel_id=1, source_target_pairs={{0,4},{4,8},{8,12},{12,16},{16,20},{20,24},{24,28},{28,0},{1,5},{5... | collective-permute-start | bytes 540680 | tf_op jit(solution)/shard_map/ppermute | solution.py:41
  210.5 9.3 %collective-permute-start.12 = (bf16[704,128]{1,0:T(8,128)(2,1)S(1)}, bf16[704,128]{1,0:T(8,128)(2,1)S(1)}, u32[]{:S(2)}, u32[]{:S(2)}) collective-permute-start(bf16[704,128]{1,0:T(8,128)(2,1)S(1)} %collective-permute-done.11), channel_id=1, source_target_pairs={{0,4},{4,8},{8,12},{12,16},{16,20},{20,24},{24,28},{28,0},{1,5},{5... | collective-permute-start | bytes 540680 | tf_op jit(solution)/shard_map/ppermute | solution.py:41
  219.7 8.2 %collective-permute-start.13 = (bf16[704,128]{1,0:T(8,128)(2,1)S(1)}, bf16[704,128]{1,0:T(8,128)(2,1)S(1)}, u32[]{:S(2)}, u32[]{:S(2)}) collective-permute-start(bf16[704,128]{1,0:T(8,128)(2,1)S(1)} %collective-permute-done.12), channel_id=1, source_target_pairs={{0,4},{4,8},{8,12},{12,16},{16,20},{20,24},{24,28},{28,0},{1,5},{5... | collective-permute-start | bytes 540680 | tf_op jit(solution)/shard_map/ppermute | solution.py:41
  228.5 42.3 %copy-start.5 = (bf16[512,1024]{1,0:T(8,128)(2,1)S(1)}, bf16[512,1024]{1,0:T(8,128)(2,1)}, u32[]{:S(2)}) copy-start(bf16[512,1024]{1,0:T(8,128)(2,1)} %all-gather.13.cloned.1.call-done) | copy-start | bytes 3145732
Sparse Core Ops, SparseCore 0:
  10.5 19.4 all-gather.6
  31.9 47.9 all-gather.8
  81.9 44.1 all-gather.10
  131.5 22.9 reduce-scatter.2
  156.4 50.6 all-gather.14
  208.5 17.1 all-gather.12
  227.8 42.9 all-gather.16
  275.8 22.9 reduce-scatter.4
